TPU v7x, 32 devices: a whole 2x2x4 slice. The times are simulated.
32 devices in a mesh: sp: 8 (over z, x), tp: 4 (over y, core).
Axes of the slice: x: 2, y: 2, z: 4, core: 2. Of those that a mesh axis runs over, the one named last changes fastest.
Arguments:
- tokens: bfloat16 [2048, 1024], P(('sp', 'tp')), may hold values from -6 to 6
- norm_gain: float32 [1024], replicated, may hold values from 0.1 to 1.9
- w_query: bfloat16 [1024, 1024], P('sp', 'tp'), may hold values from -0.1875 to 0.1875
- w_key: bfloat16 [1024, 1024], P('sp', 'tp'), may hold values from -0.1875 to 0.1875
- w_value: bfloat16 [1024, 1024], P('sp', 'tp'), may hold values from -0.1875 to 0.1875
- w_forget: bfloat16 [1024, 16], P('sp', 'tp'), may hold values from -0.375 to 0.375
- forget_offset: float32 [16], P('tp'), may hold values from 1 to 3.5
- w_out_t: bfloat16 [1024, 1024], P('sp', 'tp'), may hold values from -0.1875 to 0.1875
- out_gain: float32 [1024], replicated, may hold values from 0.1 to 1.9
Outputs:
- mixed: bfloat16 [2048, 1024], P(('sp', 'tp'))
All inputs are finite; a program needn't handle non-finite values.
Results may differ from a plain program's by a relative error of at most 0.015.
Values may be sent and summed in bfloat16 or wider, within the bound.
A program may use at most 192 MiB of HBM per device.

v0:
```python
import jax
import jax.numpy as jnp
from jax import lax
from jax.sharding import PartitionSpec as P

HEAD_DIM = 64
norm_eps = 1e-06
masked_score = -1e30


def on_whole(shard, axis, dim, work):
    return work(lax.all_gather(shard, axis, axis=dim, tiled=True), jnp.int32(0))


def over_all(section, axis, dim, turn, start):

    def gathered(part):
        return lax.all_gather(part, axis, axis=dim, tiled=True)

    return turn(start, jax.tree.map(gathered, section), jnp.int32(0))


def own_rows(portion, width, axis):
    count = width * lax.axis_size(axis)
    sent = portion(jnp.int32(0), count).astype(jnp.bfloat16)
    return lax.psum_scatter(sent, axis, scatter_dimension=0, tiled=True).astype(jnp.float32)


def rms_norm(values_in, gain_row):
    floats = values_in.astype(jnp.float32)
    scale_row = lax.rsqrt(jnp.mean(floats * floats, axis=-1, keepdims=True) + norm_eps)
    return (floats * scale_row * gain_row).astype(jnp.bfloat16)


def on_device(
    tokens, norm_gain, w_query, w_key, w_value, w_forget, forget_offset, w_out_t, out_gain
):
    normed = rms_norm(tokens, norm_gain)
    width_local = w_query.shape[1]
    heads_local = w_forget.shape[1]
    tok_block = normed.shape[0] * lax.axis_size("tp")
    total_tokens = tok_block * lax.axis_size("sp")
    full_query, full_key, full_value, full_forget, out_weight = (
        lax.all_gather(w_query, "sp", axis=0, tiled=True),
        lax.all_gather(w_key, "sp", axis=0, tiled=True),
        lax.all_gather(w_value, "sp", axis=0, tiled=True),
        lax.all_gather(w_forget, "sp", axis=0, tiled=True),
        lax.all_gather(w_out_t, "sp", axis=0, tiled=True),
    )
    joined = jnp.concatenate([full_query, full_key, full_value, full_forget], axis=1)

    def project(row_piece, first_row):
        return jnp.dot(row_piece, joined, preferred_element_type=jnp.float32)

    projected_cols = on_whole(normed, "tp", 0, project)
    head_shape = (tok_block, heads_local, HEAD_DIM)
    queries = projected_cols[:, :width_local].astype(jnp.bfloat16).reshape(head_shape)
    keys_here = (
        projected_cols[:, width_local : 2 * width_local].astype(jnp.bfloat16).reshape(head_shape)
    )
    values_here = (
        projected_cols[:, 2 * width_local : 3 * width_local]
        .astype(jnp.bfloat16)
        .reshape(head_shape)
    )
    logits = (
        projected_cols[:, 3 * width_local :] + forget_offset + jnp.log(jnp.float32(total_tokens))
    )
    log_gates = jax.nn.log_sigmoid(logits)
    all_gates = lax.all_gather(log_gates, "sp", axis=0, tiled=True)
    cumulative = jnp.cumsum(all_gates, axis=0)
    offset = lax.axis_index("sp") * tok_block
    cum_query = lax.dynamic_slice_in_dim(cumulative, offset, tok_block, 0)
    query_pos = offset + jnp.arange(tok_block, dtype=jnp.int32)
    score_scale = HEAD_DIM ** (-0.5)

    def absorb(state_now, pieces, first_row):
        run_max, run_sum, run_acc = state_now
        key_piece, value_piece = pieces
        span_len = key_piece.shape[0]
        cum_key = lax.dynamic_slice_in_dim(cumulative, first_row, span_len, 0)
        scores = (
            jnp.einsum("qhd,khd->hqk", queries, key_piece, preferred_element_type=jnp.float32)
            * score_scale
        )
        scores = scores + cum_query.T[:, :, None] - cum_key.T[:, None, :]
        key_pos = first_row + jnp.arange(span_len, dtype=jnp.int32)
        allowed = (key_pos[None, :] <= query_pos[:, None])[None]
        scores = jnp.where(allowed, scores, masked_score)
        new_max = jnp.maximum(run_max, jnp.max(scores, axis=-1))
        shares = jnp.where(allowed, jnp.exp(scores - new_max[..., None]), 0.0)
        rescale = jnp.exp(run_max - new_max)
        new_sum = run_sum * rescale + jnp.sum(shares, axis=-1)
        new_acc = run_acc * rescale[..., None] + jnp.einsum(
            "hqk,khd->hqd", shares, value_piece.astype(jnp.float32), precision=lax.Precision.HIGHEST
        )
        return (new_max, new_sum, new_acc)

    start_state = (
        jnp.full((heads_local, tok_block), masked_score, jnp.float32),
        jnp.zeros((heads_local, tok_block), jnp.float32),
        jnp.zeros((heads_local, tok_block, HEAD_DIM), jnp.float32),
    )
    run_max, run_sum, run_acc = over_all((keys_here, values_here), "sp", 0, absorb, start_state)
    attended = (
        (run_acc / run_sum[..., None])
        .transpose(1, 0, 2)
        .reshape(tok_block, width_local)
        .astype(jnp.bfloat16)
    )
    rows_mine = tokens.shape[0]

    def out_term(first_row, row_count):
        block_rows = lax.dynamic_slice_in_dim(attended, first_row, row_count, 0)
        return lax.dot_general(
            block_rows, out_weight, (((1,), (1,)), ((), ())), preferred_element_type=jnp.float32
        )

    projected = own_rows(out_term, rows_mine, "tp")
    return rms_norm(projected, out_gain)


def solution(mesh):
    return jax.shard_map(
        on_device,
        mesh=mesh,
        in_specs=(
            P(("sp", "tp"), None),
            P(),
            P("sp", "tp"),
            P("sp", "tp"),
            P("sp", "tp"),
            P("sp", "tp"),
            P("tp"),
            P("sp", "tp"),
            P(),
        ),
        out_specs=P(("sp", "tp"), None),
        check_vma=False,
    )
```

profile of v0, /device:TPU:0, one launch (start us, length us, event | category | flops | bytes accessed | tf_op | source)
XLA Modules:
  0.0 256.3 jit_solution(14113764363407624056)
XLA Ops:
  6.5 0.0 copy-start.3
  6.5 0.0 copy-start.1
  6.5 0.0 all-gather.3.cloned.1.call-start
  6.5 1.1 fusion.22
  7.6 1.0 fusion.24
  8.6 8.7 %all_gather.27 = bf16[256,1024]{1,0:T(8,128)(2,1)S(1)} all-gather(bf16[64,1024]{1,0:T(8,128)(2,1)S(1)} %fusion.24), channel_id=1, replica_groups=mesh['sp'=8,'tp'=4] {'tp'}, dimensions={0}, use_global_device_ids=true | all-gather | bytes 655360 | tf_op jit(solution)/shard_map/all_gather | solution.py:12
  17.3 32.1 %all_gather.28 = bf16[1024,256]{1,0:T(8,128)(2,1)S(1)} all-gather(bf16[128,256]{1,0:T(8,128)(2,1)} %param.11), channel_id=1, replica_groups=mesh['sp'=8,'tp'=4] {'sp'}, dimensions={0}, use_global_device_ids=true | all-gather | bytes 589824 | tf_op jit(solution)/shard_map/all_gather | solution.py:44
  49.4 31.6 %all_gather.29 = bf16[1024,256]{1,0:T(8,128)(2,1)S(1)} all-gather(bf16[128,256]{1,0:T(8,128)(2,1)} %param.12), channel_id=1, replica_groups=mesh['sp'=8,'tp'=4] {'sp'}, dimensions={0}, use_global_device_ids=true | all-gather | bytes 589824 | tf_op jit(solution)/shard_map/all_gather | solution.py:45
  81.0 31.4 %all_gather.30 = bf16[1024,256]{1,0:T(8,128)(2,1)S(1)} all-gather(bf16[128,256]{1,0:T(8,128)(2,1)} %param.13), channel_id=1, replica_groups=mesh['sp'=8,'tp'=4] {'sp'}, dimensions={0}, use_global_device_ids=true | all-gather | bytes 589824 | tf_op jit(solution)/shard_map/all_gather | solution.py:46
  112.4 21.0 %all_gather.31 = bf16[1024,4]{0,1:T(4,128)(2,1)S(1)} all-gather(bf16[128,4]{0,1:T(4,128)(2,1)} %param.14), channel_id=1, replica_groups=mesh['sp'=8,'tp'=4] {'sp'}, dimensions={0}, use_global_device_ids=true | all-gather | bytes 9216 | tf_op jit(solution)/shard_map/all_gather | solution.py:47
  133.4 0.2 copy.11
  133.6 0.8 fusion.36
  134.4 0.7 fusion.35
  135.1 0.0 all-gather.3.cloned.1.call-update
  135.2 0.0 all-gather.5.cloned.1.call-start
  135.2 0.7 all-gather.5.cloned.1.call-update
  135.9 0.0 reduce-scatter.2.cloned.1.call-start
  136.0 0.0 copy-done.3
  136.0 0.1 fusion.28
  136.1 30.9 %all_gather.33 = f32[2048,4]{0,1:T(4,128)S(1)} all-gather(f32[256,4]{0,1:T(4,128)S(1)} %fusion.28), channel_id=1, replica_groups=mesh['sp'=8,'tp'=4] {'sp'}, dimensions={0}, use_global_device_ids=true | all-gather | bytes 36864 | tf_op jit(solution)/shard_map/all_gather | solution.py:70
  167.0 1.1 reduce-window.6
  168.1 0.2 slice_reduce_fusion
  168.3 0.2 reduce-window.9
  168.5 0.1 add_bitcast_fusion
  168.6 0.4 iota_compare_fusion
  168.9 0.0 copy-done.1
  168.9 31.6 %all_gather.35 = bf16[1024,256]{1,0:T(8,128)(2,1)S(1)} all-gather(bf16[128,256]{1,0:T(8,128)(2,1)S(1)} %copy-done.1), channel_id=1, replica_groups=mesh['sp'=8,'tp'=4] {'sp'}, dimensions={0}, use_global_device_ids=true | all-gather | bytes 589824 | tf_op jit(solution)/shard_map/all_gather | solution.py:48
  200.5 0.0 all-gather.3.cloned.1.call-done
  200.5 3.9 %fusion.2 = (f32[4,256]{1,0:T(4,128)S(1)}, f32[4,256,2048]{2,1,0:T(8,128)S(1)}) fusion(f32[4,2048]{1,0:T(4,128)S(1)} %bitcast.38, f32[4,256]{1,0:T(4,128)S(1)} %constant_dynamic-slice_fusion, pred[256,2048]{1,0:T(8,128)(4,1)S(1)} %iota_compare_fusion, bf16[256,4,64]{0,2,1:T(8,128)(2,1)S(1)} %bitcast.44, bf16[2048,4,64]{0,2,1:T(8,128)(2,1)} %all-gather.3.cloned.1.call-done), kind=kOutput, calls=%fused_computation.4 | convolution fusion | flops 278920192 | bytes 10133504 | tf_op jit(solution)/shard_map/qhd,khd->hqk/dot_general | solution.py:83
  204.4 0.0 copy-start
  204.4 3.2 %copy-done = f32[4,256,2048]{2,1,0:T(8,128)} copy-done((f32[4,256,2048]{2,1,0:T(8,128)}, f32[4,256,2048]{2,1,0:T(8,128)S(1)}, u32[]{:S(2)}) %copy-start) | copy-done | bytes 8388632
  207.6 3.2 %fusion = f32[4,256]{1,0:T(4,128)S(1)} fusion(f32[4,256,2048]{2,1,0:T(8,128)S(1)} %get-tuple-element.13, f32[4,256]{1,0:T(4,128)S(1)} %get-tuple-element.9, f32[4,2048]{1,0:T(4,128)S(1)} %bitcast.39, f32[4,256]{1,0:T(4,128)S(1)} %constant_dynamic-slice_fusion, pred[256,2048]{1,0:T(8,128)(4,1)S(1)} %iota_compare_fusion), kind=kLoop, calls=%fused_computation.2 | loop fusion | flops 14679040 | bytes 8957952 | tf_op jit(solution)/shard_map/reduce_sum | solution.py:93
  210.8 3.8 %all-gather.5.cloned.1.call-done = bf16[2048,4,64]{0,2,1:T(8,128)(2,1)} async-done(((bf16[256,4,64]{0,2,1:T(8,128)(2,1)}), bf16[2048,4,64]{0,2,1:T(8,128)(2,1)}) %all-gather.5.cloned.1.call-update) | async-done | bytes 1048592 | tf_op jit(solution)/shard_map/all_gather | solution.py:18
  214.7 0.0 copy-start.2
  214.7 10.4 %fusion.21 = bf16[256,4,64]{0,2,1:T(8,128)(2,1)S(1)} fusion(bf16[2048,4,64]{0,2,1:T(8,128)(2,1)} %all-gather.5.cloned.1.call-done, f32[4,256,2048]{2,1,0:T(8,128)} %copy-done, f32[4,256]{1,0:T(4,128)S(1)} %get-tuple-element.9, f32[4,2048]{1,0:T(4,128)S(1)} %bitcast.40, f32[4,256]{1,0:T(4,128)S(1)} %constant_dynamic-slice_fusion, ...), kind=kOutput, calls=%fused_computation.25 | convolution fusion | flops 1623392256 | bytes 10141696 | tf_op jit(solution)/shard_map/hqk,khd->hqd/dot_general | solution.py:94
  225.1 1.2 convolution_convert_fusion
  226.2 0.0 reduce-scatter.2.cloned.1.call-update
  226.2 20.9 %reduce-scatter.2.cloned.1.call-done = bf16[64,1024]{1,0:T(8,128)(2,1)} async-done(((bf16[256,1024]{1,0:T(8,128)(2,1)}), bf16[64,1024]{1,0:T(8,128)(2,1)}) %reduce-scatter.2.cloned.1.call-update) | async-done | bytes 131088 | tf_op jit(solution)/shard_map/reduce_scatter | solution.py:26
  247.1 1.0 fusion.25
  248.1 0.0 copy-done.2
  248.2 1.7 fusion.27
  (8 shorter events, 0.1 us)
Async XLA Ops:
  6.5 129.5 %copy-start.3 = (f32[4]{0:T(128)S(1)}, f32[4]{0:T(128)}, u32[]{:S(2)}) copy-start(f32[4]{0:T(128)} %param.15) | copy-start | bytes 52
  6.5 162.4 %copy-start.1 = (bf16[128,256]{1,0:T(8,128)(2,1)S(1)}, bf16[128,256]{1,0:T(8,128)(2,1)}, u32[]{:S(2)}) copy-start(bf16[128,256]{1,0:T(8,128)(2,1)} %param.16) | copy-start | bytes 196612
  6.5 194.0 %all-gather.3.cloned.1.call-start = ((), (), s32[]{:S(2)}) async-start(), calls=%async_computation.1 | async-start | bytes 1179648 | tf_op jit(solution)/shard_map/all_gather | solution.py:18
  135.2 79.5 %all-gather.5.cloned.1.call-start = ((), (), s32[]{:S(2)}) async-start(), calls=%async_computation.2 | async-start | bytes 1179648 | tf_op jit(solution)/shard_map/all_gather | solution.py:18
  135.9 111.2 %reduce-scatter.2.cloned.1.call-start = ((), (), s32[]{:S(2)}) async-start(), calls=%async_computation.3 | async-start | bytes 655360 | tf_op jit(solution)/shard_map/reduce_scatter | solution.py:26
  204.4 3.2 %copy-start = (f32[4,256,2048]{2,1,0:T(8,128)}, f32[4,256,2048]{2,1,0:T(8,128)S(1)}, u32[]{:S(2)}) copy-start(f32[4,256,2048]{2,1,0:T(8,128)S(1)} %get-tuple-element.13) | copy-start | bytes 25165828
  214.7 33.5 %copy-start.2 = (f32[1024]{0:T(1024)S(1)}, f32[1024]{0:T(1024)}, u32[]{:S(2)}) copy-start(f32[1024]{0:T(1024)} %param.17) | copy-start | bytes 12292
Sparse Core Ops, SparseCore 0:
  135.3 37.4 all-gather.2
  174.8 39.7 all-gather.4
  226.4 20.6 reduce-scatter.1
where the time goes:
time: 257 us; the launch traced here: 256 us
  blocking collectives  187 us (73%)
  waiting for transfers between devices  25.4 us (10%)
  matrix products  16.2 us (6%)
  between operations  13.2 us (5%)
  other arithmetic  9.86 us (4%)
  local copies, waits for them, and re-layouts  4.32 us (2%)
    all_gather x1, blocking collectives, on_device(): lax.all_gather(w_query, 'sp', axis=0, tiled=True)  32.1 us
    all_gather x1, blocking collectives, on_device(): lax.all_gather(w_key, 'sp', axis=0, tiled=True)  31.6 us
    all_gather x1, blocking collectives, on_device(): lax.all_gather(w_out_t, 'sp', axis=0, tiled=True)  31.6 us
    all_gather x1, blocking collectives, on_device(): lax.all_gather(w_value, 'sp', axis=0, tiled=True)  31.4 us
    all_gather x1, blocking collectives, on_device(): all_gates = lax.all_gather(log_gates, 'sp', axis=0, tiled=True)  30.9 us
    all_gather x1, blocking collectives, on_device(): lax.all_gather(w_forget, 'sp', axis=0, tiled=True)  21 us
    reduce_scatter x1, waiting for transfers between devices, own_rows(): lax.psum_scatter(sent, axis, scatter_dimension=0, tiled=True)  20.9 us
    dot_general x1, matrix products, absorb(): jnp.einsum('hqk,khd->hqd', shares, value_piece.astype(jnp.float32), preci...  10.4 us
  transfers between devices with their start and end apart: 3, of which 2 were waited for; matrix products, arithmetic and copies ran while one was open for 4% of the time, Pallas kernels for 0%

commit v1 on v0

--- a/solution.py
+++ b/solution.py
@@ -67,7 +67,12 @@
         projected_cols[:, 3 * width_local :] + forget_offset + jnp.log(jnp.float32(total_tokens))
     )
     log_gates = jax.nn.log_sigmoid(logits)
-    all_gates = lax.all_gather(log_gates, "sp", axis=0, tiled=True)
+    ring = [log_gates]
+    for hop in range(7):
+        ring.append(lax.ppermute(ring[-1], "sp", [(dev, (dev + 1) % 8) for dev in range(8)]))
+    all_gates = jnp.roll(
+        jnp.concatenate(ring[::-1], axis=0), (lax.axis_index("sp") + 1) * ring[0].shape[0], axis=0
+    )
     cumulative = jnp.cumsum(all_gates, axis=0)
     offset = lax.axis_index("sp") * tok_block
     cum_query = lax.dynamic_slice_in_dim(cumulative, offset, tok_block, 0)

time: 257 us -> 262 us (1.019)
  waiting for transfers between devices: 25.4 us -> 60.5 us
  blocking collectives: 187 us -> 157 us
    ppermute x0 -> x7, waiting for transfers between devices: none -> 37.7 us  [on_device(): lax.ppermute(ring[-1], 'sp', [(dev, (dev + 1) % 8) for dev in range(8)])]
    all_gather x1 -> x0, blocking collectives: 30.9 us -> none  [on_device(): all_gates = lax.all_gather(log_gates, 'sp', axis=0, tiled=True)]
    all_gather x2, waiting for transfers between devices: 3.82 us -> 0.04 us  [gathered(): return lax.all_gather(part, axis, axis=dim, tiled=True)]
  transfers between devices with their start and end apart: 3 -> 10, of which waited for: 2 -> 7; matrix products, arithmetic and copies ran while one was open for 4% -> 4% of each run, Pallas kernels for 0% -> 0%
where the time goes in v1:
time: 262 us; the launch traced here: 261 us
  blocking collectives  157 us (60%)
  waiting for transfers between devices  60.5 us (23%)
  matrix products  16.2 us (6%)
  between operations  13.3 us (5%)
  other arithmetic  10.1 us (4%)
  local copies, waits for them, and re-layouts  4.46 us (2%)
    ppermute x7, waiting for transfers between devices, on_device(): lax.ppermute(ring[-1], 'sp', [(dev, (dev + 1) % 8) for dev in range(8)])  37.7 us
    all_gather x1, blocking collectives, on_device(): lax.all_gather(w_query, 'sp', axis=0, tiled=True)  32.1 us
    all_gather x1, blocking collectives, on_device(): lax.all_gather(w_out_t, 'sp', axis=0, tiled=True)  31.8 us
    all_gather x1, blocking collectives, on_device(): lax.all_gather(w_key, 'sp', axis=0, tiled=True)  31.6 us
    all_gather x1, blocking collectives, on_device(): lax.all_gather(w_value, 'sp', axis=0, tiled=True)  31.4 us
    reduce_scatter x1, waiting for transfers between devices, own_rows(): lax.psum_scatter(sent, axis, scatter_dimension=0, tiled=True)  22.8 us
    all_gather x1, blocking collectives, on_device(): lax.all_gather(w_forget, 'sp', axis=0, tiled=True)  21 us
    dot_general x1, matrix products, absorb(): jnp.einsum('hqk,khd->hqd', shares, value_piece.astype(jnp.float32), preci...  10.4 us
  transfers between devices with their start and end apart: 10, of which 7 were waited for; matrix products, arithmetic and copies ran while one was open for 4% of the time, Pallas kernels for 0%

profile of v1, /device:TPU:0, one launch (start us, length us, event | category | flops | bytes accessed | tf_op | source)
XLA Modules:
  0.0 261.3 jit_solution(3001031216255157700)
XLA Ops:
  6.5 1.1 fusion.22
  7.6 1.0 fusion.24
  8.6 8.7 %all_gather.24 = bf16[256,1024]{1,0:T(8,128)(2,1)S(1)} all-gather(bf16[64,1024]{1,0:T(8,128)(2,1)S(1)} %fusion.24), channel_id=1, replica_groups=mesh['sp'=8,'tp'=4] {'tp'}, dimensions={0}, use_global_device_ids=true | all-gather | bytes 655360 | tf_op jit(solution)/shard_map/all_gather | solution.py:12
  17.3 32.1 %all_gather.25 = bf16[1024,256]{1,0:T(8,128)(2,1)S(1)} all-gather(bf16[128,256]{1,0:T(8,128)(2,1)} %param.11), channel_id=1, replica_groups=mesh['sp'=8,'tp'=4] {'sp'}, dimensions={0}, use_global_device_ids=true | all-gather | bytes 589824 | tf_op jit(solution)/shard_map/all_gather | solution.py:44
  49.4 31.6 %all_gather.26 = bf16[1024,256]{1,0:T(8,128)(2,1)S(1)} all-gather(bf16[128,256]{1,0:T(8,128)(2,1)} %param.12), channel_id=1, replica_groups=mesh['sp'=8,'tp'=4] {'sp'}, dimensions={0}, use_global_device_ids=true | all-gather | bytes 589824 | tf_op jit(solution)/shard_map/all_gather | solution.py:45
  81.0 31.4 %all_gather.27 = bf16[1024,256]{1,0:T(8,128)(2,1)S(1)} all-gather(bf16[128,256]{1,0:T(8,128)(2,1)} %param.13), channel_id=1, replica_groups=mesh['sp'=8,'tp'=4] {'sp'}, dimensions={0}, use_global_device_ids=true | all-gather | bytes 589824 | tf_op jit(solution)/shard_map/all_gather | solution.py:46
  112.4 21.0 %all_gather.28 = bf16[1024,4]{0,1:T(4,128)(2,1)S(1)} all-gather(bf16[128,4]{0,1:T(4,128)(2,1)} %param.14), channel_id=1, replica_groups=mesh['sp'=8,'tp'=4] {'sp'}, dimensions={0}, use_global_device_ids=true | all-gather | bytes 9216 | tf_op jit(solution)/shard_map/all_gather | solution.py:47
  133.4 0.2 copy.11
  133.6 0.8 fusion.36
  134.4 0.7 fusion.35
  135.1 0.0 all-gather.3.cloned.1.call-update
  135.2 0.0 all-gather.5.cloned.1.call-start
  135.2 0.1 fusion.28
  135.3 0.1 collective-permute-start
  135.4 6.3 %collective-permute-done = f32[256,4]{0,1:T(4,128)S(1)} collective-permute-done((f32[256,4]{0,1:T(4,128)S(1)}, f32[256,4]{0,1:T(4,128)S(1)}, u32[]{:S(2)}, u32[]{:S(2)}) %collective-permute-start) | collective-permute-done | bytes 4128 | tf_op jit(solution)/shard_map/ppermute | solution.py:72
  141.7 0.0 collective-permute-start.1
  141.7 6.3 %collective-permute-done.1 = f32[256,4]{0,1:T(4,128)S(1)} collective-permute-done((f32[256,4]{0,1:T(4,128)S(1)}, f32[256,4]{0,1:T(4,128)S(1)}, u32[]{:S(2)}, u32[]{:S(2)}) %collective-permute-start.1) | collective-permute-done | bytes 4128 | tf_op jit(solution)/shard_map/ppermute | solution.py:72
  148.0 0.0 collective-permute-start.2
  148.0 6.3 %collective-permute-done.2 = f32[256,4]{0,1:T(4,128)S(1)} collective-permute-done((f32[256,4]{0,1:T(4,128)S(1)}, f32[256,4]{0,1:T(4,128)S(1)}, u32[]{:S(2)}, u32[]{:S(2)}) %collective-permute-start.2) | collective-permute-done | bytes 4128 | tf_op jit(solution)/shard_map/ppermute | solution.py:72
  154.3 0.0 collective-permute-start.3
  154.3 0.0 all-gather.5.cloned.1.call-update
  154.3 0.0 reduce-scatter.2.cloned.1.call-start
  154.4 6.3 %collective-permute-done.3 = f32[256,4]{0,1:T(4,128)S(1)} collective-permute-done((f32[256,4]{0,1:T(4,128)S(1)}, f32[256,4]{0,1:T(4,128)S(1)}, u32[]{:S(2)}, u32[]{:S(2)}) %collective-permute-start.3) | collective-permute-done | bytes 4128 | tf_op jit(solution)/shard_map/ppermute | solution.py:72
  160.7 6.4 %collective-permute-done.4 = f32[256,4]{0,1:T(4,128)S(1)} collective-permute-done((f32[256,4]{0,1:T(4,128)S(1)}, f32[256,4]{0,1:T(4,128)S(1)}, u32[]{:S(2)}, u32[]{:S(2)}) %collective-permute-start.4) | collective-permute-done | bytes 4128 | tf_op jit(solution)/shard_map/ppermute | solution.py:72
  167.1 0.0 collective-permute-start.5
  167.1 0.4 iota_compare_fusion
  167.5 6.0 %collective-permute-done.5 = f32[256,4]{0,1:T(4,128)S(1)} collective-permute-done((f32[256,4]{0,1:T(4,128)S(1)}, f32[256,4]{0,1:T(4,128)S(1)}, u32[]{:S(2)}, u32[]{:S(2)}) %collective-permute-start.5) | collective-permute-done | bytes 4128 | tf_op jit(solution)/shard_map/ppermute | solution.py:72
  173.5 0.0 collective-permute-start.6
  173.5 31.8 %all_gather.31 = bf16[1024,256]{1,0:T(8,128)(2,1)S(1)} all-gather(bf16[128,256]{1,0:T(8,128)(2,1)S(1)} %copy-done.1), channel_id=1, replica_groups=mesh['sp'=8,'tp'=4] {'sp'}, dimensions={0}, use_global_device_ids=true | all-gather | bytes 589824 | tf_op jit(solution)/shard_map/all_gather | solution.py:48
  205.3 0.0 collective-permute-done.6
  205.4 0.1 constant_dynamic-update-slice_fusion.8
  205.6 0.1 constant_dynamic-update-slice_fusion
  205.7 1.2 reduce-window.6
  206.9 0.2 slice_reduce_fusion
  207.0 0.2 reduce-window.9
  207.2 0.1 add_bitcast_fusion
  207.4 0.0 all-gather.3.cloned.1.call-done
  207.4 3.8 %fusion.2 = (f32[4,256]{1,0:T(4,128)S(1)}, f32[4,256,2048]{2,1,0:T(8,128)S(1)}) fusion(f32[4,2048]{1,0:T(4,128)S(1)} %bitcast.39, f32[4,256]{1,0:T(4,128)S(1)} %constant_dynamic-slice_fusion, pred[256,2048]{1,0:T(8,128)(4,1)S(1)} %iota_compare_fusion, bf16[256,4,64]{0,2,1:T(8,128)(2,1)S(1)} %bitcast.44, bf16[2048,4,64]{0,2,1:T(8,128)(2,1)} %all-gather.3.cloned.1.call-done), kind=kOutput, calls=%fused_computation.4 | convolution fusion | flops 278920192 | bytes 10133504 | tf_op jit(solution)/shard_map/qhd,khd->hqk/dot_general | solution.py:88
  211.3 3.2 %copy-done = f32[4,256,2048]{2,1,0:T(8,128)} copy-done((f32[4,256,2048]{2,1,0:T(8,128)}, f32[4,256,2048]{2,1,0:T(8,128)S(1)}, u32[]{:S(2)}) %copy-start) | copy-done | bytes 8388632
  214.5 3.2 %fusion = f32[4,256]{1,0:T(4,128)S(1)} fusion(f32[4,256,2048]{2,1,0:T(8,128)S(1)} %get-tuple-element.13, f32[4,256]{1,0:T(4,128)S(1)} %get-tuple-element.9, f32[4,2048]{1,0:T(4,128)S(1)} %bitcast.40, f32[4,256]{1,0:T(4,128)S(1)} %constant_dynamic-slice_fusion, pred[256,2048]{1,0:T(8,128)(4,1)S(1)} %iota_compare_fusion), kind=kLoop, calls=%fused_computation.2 | loop fusion | flops 14679040 | bytes 8957952 | tf_op jit(solution)/shard_map/reduce_sum | solution.py:98
  217.7 0.0 all-gather.5.cloned.1.call-done
  217.7 0.0 copy-start.3
  217.7 10.4 %fusion.21 = bf16[256,4,64]{0,2,1:T(8,128)(2,1)S(1)} fusion(bf16[2048,4,64]{0,2,1:T(8,128)(2,1)} %all-gather.5.cloned.1.call-done, f32[4,256,2048]{2,1,0:T(8,128)} %copy-done, f32[4,256]{1,0:T(4,128)S(1)} %get-tuple-element.9, f32[4,2048]{1,0:T(4,128)S(1)} %bitcast.41, f32[4,256]{1,0:T(4,128)S(1)} %constant_dynamic-slice_fusion, ...), kind=kOutput, calls=%fused_computation.25 | convolution fusion | flops 1623392256 | bytes 10141696 | tf_op jit(solution)/shard_map/hqk,khd->hqd/dot_general | solution.py:99
  228.1 1.1 convolution_convert_fusion
  229.3 0.0 reduce-scatter.2.cloned.1.call-update
  229.3 22.8 %reduce-scatter.2.cloned.1.call-done = bf16[64,1024]{1,0:T(8,128)(2,1)} async-done(((bf16[256,1024]{1,0:T(8,128)(2,1)}), bf16[64,1024]{1,0:T(8,128)(2,1)}) %reduce-scatter.2.cloned.1.call-update) | async-done | bytes 131088 | tf_op jit(solution)/shard_map/reduce_scatter | solution.py:26
  252.0 1.0 fusion.25
  253.1 1.7 fusion.27
  (31 shorter events, 0.2 us)
Async XLA Ops:
  6.5 128.7 %copy-start.2 = (f32[4]{0:T(128)S(1)}, f32[4]{0:T(128)}, u32[]{:S(2)}) copy-start(f32[4]{0:T(128)} %param.15) | copy-start | bytes 52
  6.5 167.0 %copy-start.1 = (bf16[128,256]{1,0:T(8,128)(2,1)S(1)}, bf16[128,256]{1,0:T(8,128)(2,1)}, u32[]{:S(2)}) copy-start(bf16[128,256]{1,0:T(8,128)(2,1)} %param.16) | copy-start | bytes 196612
  6.5 200.8 %all-gather.3.cloned.1.call-start = ((), (), s32[]{:S(2)}) async-start(), calls=%async_computation.1 | async-start | bytes 1179648 | tf_op jit(solution)/shard_map/all_gather | solution.py:18
  135.2 82.5 %all-gather.5.cloned.1.call-start = ((), (), s32[]{:S(2)}) async-start(), calls=%async_computation.2 | async-start | bytes 1179648 | tf_op jit(solution)/shard_map/all_gather | solution.py:18
  135.3 6.4 %collective-permute-start = (f32[256,4]{0,1:T(4,128)S(1)}, f32[256,4]{0,1:T(4,128)S(1)}, u32[]{:S(2)}, u32[]{:S(2)}) collective-permute-start(f32[256,4]{0,1:T(4,128)S(1)} %fusion.28), channel_id=1, source_target_pairs={{0,4},{4,8},{8,12},{12,16},{16,20},{20,24},{24,28},{28,0},{1,5},{5... | collective-permute-start | bytes 12296 | tf_op jit(solution)/shard_map/ppermute | solution.py:72
  141.7 6.3 %collective-permute-start.1 = (f32[256,4]{0,1:T(4,128)S(1)}, f32[256,4]{0,1:T(4,128)S(1)}, u32[]{:S(2)}, u32[]{:S(2)}) collective-permute-start(f32[256,4]{0,1:T(4,128)S(1)} %collective-permute-done), channel_id=1, source_target_pairs={{0,4},{4,8},{8,12},{12,16},{16,20},{20,24},{24,28},{28,0},{1,5},{5... | collective-permute-start | bytes 12296 | tf_op jit(solution)/shard_map/ppermute | solution.py:72
  148.0 6.3 %collective-permute-start.2 = (f32[256,4]{0,1:T(4,128)S(1)}, f32[256,4]{0,1:T(4,128)S(1)}, u32[]{:S(2)}, u32[]{:S(2)}) collective-permute-start(f32[256,4]{0,1:T(4,128)S(1)} %collective-permute-done.1), channel_id=1, source_target_pairs={{0,4},{4,8},{8,12},{12,16},{16,20},{20,24},{24,28},{28,0},{1,5},{5... | collective-permute-start | bytes 12296 | tf_op jit(solution)/shard_map/ppermute | solution.py:72
  154.3 6.4 %collective-permute-start.3 = (f32[256,4]{0,1:T(4,128)S(1)}, f32[256,4]{0,1:T(4,128)S(1)}, u32[]{:S(2)}, u32[]{:S(2)}) collective-permute-start(f32[256,4]{0,1:T(4,128)S(1)} %collective-permute-done.2), channel_id=1, source_target_pairs={{0,4},{4,8},{8,12},{12,16},{16,20},{20,24},{24,28},{28,0},{1,5},{5... | collective-permute-start | bytes 12296 | tf_op jit(solution)/shard_map/ppermute | solution.py:72
  154.3 97.7 %reduce-scatter.2.cloned.1.call-start = ((), (), s32[]{:S(2)}) async-start(), calls=%async_computation.3 | async-start | bytes 655360 | tf_op jit(solution)/shard_map/reduce_scatter | solution.py:26
  160.7 6.4 %collective-permute-start.4 = (f32[256,4]{0,1:T(4,128)S(1)}, f32[256,4]{0,1:T(4,128)S(1)}, u32[]{:S(2)}, u32[]{:S(2)}) collective-permute-start(f32[256,4]{0,1:T(4,128)S(1)} %collective-permute-done.3), channel_id=1, source_target_pairs={{0,4},{4,8},{8,12},{12,16},{16,20},{20,24},{24,28},{28,0},{1,5},{5... | collective-permute-start | bytes 12296 | tf_op jit(solution)/shard_map/ppermute | solution.py:72
  167.1 6.4 %collective-permute-start.5 = (f32[256,4]{0,1:T(4,128)S(1)}, f32[256,4]{0,1:T(4,128)S(1)}, u32[]{:S(2)}, u32[]{:S(2)}) collective-permute-start(f32[256,4]{0,1:T(4,128)S(1)} %collective-permute-done.4), channel_id=1, source_target_pairs={{0,4},{4,8},{8,12},{12,16},{16,20},{20,24},{24,28},{28,0},{1,5},{5... | collective-permute-start | bytes 12296 | tf_op jit(solution)/shard_map/ppermute | solution.py:72
  173.5 31.8 %collective-permute-start.6 = (f32[256,4]{0,1:T(4,128)S(1)}, f32[256,4]{0,1:T(4,128)S(1)}, u32[]{:S(2)}, u32[]{:S(2)}) collective-permute-start(f32[256,4]{0,1:T(4,128)S(1)} %collective-permute-done.5), channel_id=1, source_target_pairs={{0,4},{4,8},{8,12},{12,16},{16,20},{20,24},{24,28},{28,0},{1,5},{5... | collective-permute-start | bytes 12296 | tf_op jit(solution)/shard_map/ppermute | solution.py:72
  211.2 3.2 %copy-start = (f32[4,256,2048]{2,1,0:T(8,128)}, f32[4,256,2048]{2,1,0:T(8,128)S(1)}, u32[]{:S(2)}) copy-start(f32[4,256,2048]{2,1,0:T(8,128)S(1)} %get-tuple-element.13) | copy-start | bytes 25165828
  217.7 35.4 %copy-start.3 = (f32[1024]{0:T(1024)S(1)}, f32[1024]{0:T(1024)}, u32[]{:S(2)}) copy-start(f32[1024]{0:T(1024)} %param.17) | copy-start | bytes 12292
Sparse Core Ops, SparseCore 0:
  135.3 37.2 all-gather.2
  174.6 38.7 all-gather.4
  229.4 22.5 reduce-scatter.1
